TPU v7x, 32 devices: a whole 2x2x4 slice. The times are simulated.
32 devices in a mesh: kv: 8 (over z, y), tp: 4 (over x, core).
Axes of the slice: x: 2, y: 2, z: 4, core: 2. Of those that a mesh axis runs over, the one named last changes fastest.
Arguments:
- tokens: bfloat16 [4096, 2048], P('kv', 'tp'), may hold values from -9 to 9
- w_query: bfloat16 [2048, 1536], P(None, 'tp'), may hold values from -1 to 1
- w_key: bfloat16 [2048, 1536], P(None, 'tp'), may hold values from -1 to 1
- w_value: bfloat16 [2048, 1536], P(None, 'tp'), may hold values from -0.5 to 0.5
- w_out: bfloat16 [1536, 2048], P('tp'), may hold values from -0.15625 to 0.15625
- chosen: int32 [128, 24], P('kv'), may hold values from 0 to 127, as said below
Outputs:
- mixed: bfloat16 [4096, 2048], P(('kv', 'tp'))
Inputs may be any that keep to these rules, and one draw needn't show every extreme that they name: `chosen`: row c names blocks no later than c; its first entry is c and its second c - 1 (0 for row 0), and an entry may repeat. Taking the rows in aligned runs of 16, one run for each index of kv, the rows of one run name at most 2 distinct blocks lying in any one other index's positions; in every draw some index of kv names exactly 2 from every earlier index. Every run names some block of the index just before it and of the index half the axis before it, where those exist.
All inputs are finite; a program needn't handle non-finite values.
Results may differ from a plain program's by a relative error of at most 0.014.
Values may be sent and summed in bfloat16 or wider, within the bound.
A program may use at most 320 MiB of HBM per device.

v0:
```python
import jax
import jax.numpy as jnp
from jax import lax
from jax.sharding import PartitionSpec as P

HD = 128
BLK = 32
MOST = 2


NEG = -1e30


def attend(query_rows, key_rows, value_rows, block_ids, chosen, first_block):
    tok_rows, width = query_rows.shape
    head_count = width // HD
    key_count = key_rows.shape[0]
    slot_count = key_count // BLK
    query_blocks = tok_rows // BLK
    seen = (
        jnp.any(chosen[:, :, None] == block_ids[None, None, :], axis=1) & (block_ids >= 0)[None, :]
    )
    grid = jnp.broadcast_to(seen[:, None, :, None], (query_blocks, BLK, slot_count, BLK)).reshape(
        tok_rows, key_count
    )
    key_pos = (block_ids[:, None] * BLK + jnp.arange(BLK, dtype=jnp.int32)[None, :]).reshape(
        key_count
    )
    query_pos = first_block * BLK + jnp.arange(tok_rows, dtype=jnp.int32)
    allowed = grid & (key_pos[None, :] <= query_pos[:, None])
    query_heads = query_rows.reshape(tok_rows, head_count, HD)
    key_heads = key_rows.reshape(key_count, head_count, HD)
    value_heads = value_rows.reshape(key_count, head_count, HD)
    scores = jnp.einsum(
        "qhd,khd->hqk", query_heads, key_heads, preferred_element_type=jnp.float32
    ) * HD ** (-0.5)
    scores = jnp.where(allowed[None], scores, NEG)
    highest = jnp.max(scores, axis=-1)
    weights = jnp.where(allowed[None], jnp.exp(scores - highest[..., None]), 0.0)
    totals = jnp.sum(weights, axis=-1)
    summed = jnp.einsum("hqk,khd->hqd", weights, value_heads.astype(jnp.float32))
    return (highest, totals, summed)


def combine(left, right):
    highest = jnp.maximum(left[0], right[0])
    left_scale = jnp.exp(left[0] - highest)
    right_scale = jnp.exp(right[0] - highest)
    totals = left[1] * left_scale + right[1] * right_scale
    summed = left[2] * left_scale[..., None] + right[2] * right_scale[..., None]
    return (highest, totals, summed)


def local(tokens, w_query, w_key, w_value, w_out, chosen):
    tok_rows = tokens.shape[0]
    width = w_query.shape[1]
    empty = jnp.zeros((tok_rows, width), jnp.float32)
    totals = (empty, empty, empty)
    piece = lax.all_gather(tokens, "tp", axis=1, tiled=True)
    outputs = []
    for total, weight in zip(totals, (w_query, w_key, w_value)):
        rows = weight
        outputs.append(jnp.dot(piece, rows, preferred_element_type=jnp.float32))
    query_full, key_full, value_full = tuple(outputs)
    query_rows = query_full.astype(jnp.bfloat16)
    key_rows = key_full.astype(jnp.bfloat16)
    value_rows = value_full.astype(jnp.bfloat16)
    per_dev = tok_rows // BLK
    my_index = lax.axis_index("kv")
    first_block = my_index * per_dev
    own_ids = first_block + jnp.arange(per_dev, dtype=jnp.int32)
    own_part = attend(query_rows, key_rows, value_rows, own_ids, chosen, first_block)
    peers = lax.axis_size("kv")
    block_total = peers * per_dev
    wanted = jnp.any(
        chosen[:, :, None] == jnp.arange(block_total, dtype=jnp.int32)[None, None, :], axis=(0, 1)
    )
    peer_ids = jnp.arange(peers, dtype=jnp.int32)
    wanted = wanted.reshape(peers, per_dev) & (peer_ids != my_index)[:, None]
    ranks = jnp.cumsum(wanted.astype(jnp.int32), axis=1) - 1
    slot_hit = wanted[:, :, None] & (
        ranks[:, :, None] == jnp.arange(MOST, dtype=jnp.int32)[None, None, :]
    )
    local_ids = jnp.sum(
        slot_hit.astype(jnp.int32) * jnp.arange(per_dev, dtype=jnp.int32)[None, :, None], axis=1
    )
    present = jnp.any(slot_hit, axis=1)
    request = jnp.where(present, local_ids, -1)
    asked = lax.all_to_all(request, "kv", split_axis=0, concat_axis=0, tiled=True)
    picked = jnp.clip(asked, 0).reshape(-1)
    send_keys = key_rows.reshape(per_dev, BLK, width)[picked]
    send_values = value_rows.reshape(per_dev, BLK, width)[picked]
    got_keys, got_values = (
        lax.all_to_all(send_keys, "kv", split_axis=0, concat_axis=0, tiled=True),
        lax.all_to_all(send_values, "kv", split_axis=0, concat_axis=0, tiled=True),
    )
    got_ids = jnp.where(present, peer_ids[:, None] * per_dev + local_ids, -1).reshape(-1)
    far_part = attend(
        query_rows,
        got_keys.reshape(-1, width),
        got_values.reshape(-1, width),
        got_ids,
        chosen,
        first_block,
    )
    merged = combine(own_part, far_part)
    normed = merged[2] / merged[1][..., None]
    attended = jnp.transpose(normed, (1, 0, 2)).reshape(tok_rows, width).astype(jnp.bfloat16)
    rows = attended
    return lax.psum_scatter(
        jnp.dot(rows, w_out, preferred_element_type=jnp.float32).astype(jnp.bfloat16),
        "tp",
        scatter_dimension=0,
        tiled=True,
    )


def solution(mesh):
    return jax.shard_map(
        local,
        mesh=mesh,
        in_specs=(
            P("kv", "tp"),
            P(None, "tp"),
            P(None, "tp"),
            P(None, "tp"),
            P("tp", None),
            P("kv", None),
        ),
        out_specs=P(("kv", "tp"), None),
        check_vma=False,
    )
```

profile of v0, /device:TPU:0, one launch (start us, length us, event | category | flops | bytes accessed | tf_op | source)
XLA Modules:
  0.0 118.5 jit_solution(13071488536581529827)
XLA Ops:
  6.5 0.0 copy-start
  6.5 0.0 all-gather.2.cloned.1.call-start
  6.5 0.7 all-gather.2.cloned.1.call-update
  7.3 0.8 fusion.26
  8.1 0.1 reshape.337
  8.2 0.1 fusion.40
  8.3 0.2 reduce_window_sum.11
  8.4 0.2 fusion.31
  8.6 0.2 select_reduce_fusion
  8.8 0.7 copy.46
  9.4 7.3 %all-to-all-start = ((s32[8,1,2]{2,1,0:T(1,128)}), s32[8,1,2]{2,1,0:T(1,128)S(1)}, u32[]{:S(2)}, u32[]{:S(2)}) async-start(s32[8,1,2]{2,1,0:T(1,128)} %copy.46), calls=%async_computation | async-start | bytes 8192 | tf_op jit(solution)/shard_map/all_to_all | solution.py:89
  16.7 0.1 copy.44
  16.8 0.1 select_n.53
  16.9 1.4 %compare_reduce_fusion = (pred[16,16]{1,0:T(8,128)(4,1)S(1)}, pred[16,16]{1,0:T(8,128)(4,1)S(1)}) fusion(s32[16,24]{1,0:T(8,128)} %param.11, s32[16]{0:T(128)S(1)} %select_n.53, s32[16]{0:T(128)S(1)} %get-tuple-element.20), kind=kLoop, calls=%fused_computation.40 | loop fusion | flops 24064 | bytes 2176 | tf_op jit(solution)/shard_map/reduce_or | solution.py:21
  18.3 0.1 copy.45
  18.4 0.3 broadcast_in_dim.42
  18.8 2.1 %reshape.338 = pred[512,512]{0,1:T(8,128)(4,1)S(1)} reshape(pred[16,32,16,32]{1,0,3,2:T(8,128)(4,1)S(1)} %broadcast_in_dim.42) | data formatting | bytes 524288 | tf_op jit(solution)/shard_map/reshape | solution.py:23
  20.9 0.1 iota_add_fusion
  21.0 0.1 add.128
  21.1 0.1 copy.38
  21.2 0.3 broadcast_in_dim.37
  21.5 2.1 %reshape.333 = pred[512,512]{0,1:T(8,128)(4,1)S(1)} reshape(pred[16,32,16,32]{1,0,3,2:T(8,128)(4,1)S(1)} %broadcast_in_dim.37) | data formatting | bytes 524288 | tf_op jit(solution)/shard_map/reshape | solution.py:23
  23.6 0.1 iota_add_fusion.1
  23.7 0.1 add.120
  23.8 0.5 compare_and_fusion
  24.3 0.0 all-to-all-done
  24.3 0.1 reshape.343
  24.4 9.8 %all-gather.2.cloned.1.call-done = bf16[512,2048]{1,0:T(8,128)(2,1)} async-done(((bf16[512,512]{1,0:T(8,128)(2,1)}), bf16[512,2048]{1,0:T(8,128)(2,1)}) %all-gather.2.cloned.1.call-update) | async-done | bytes 2097168 | tf_op jit(solution)/shard_map/all_gather | solution.py:59
  34.2 3.3 %convolution_convert_fusion.1 = bf16[512,384]{1,0:T(8,128)(2,1)S(1)} fusion(bf16[512,2048]{1,0:T(8,128)(2,1)} %all-gather.2.cloned.1.call-done, bf16[2048,384]{1,0:T(8,128)(2,1)} %param.9), kind=kOutput, calls=%fused_computation.28 | convolution fusion | flops 805502976 | bytes 4063232 | tf_op jit(solution)/shard_map/dot_general | solution.py:63
  37.5 0.9 copy.42
  38.4 3.3 %convolution_convert_fusion.2 = bf16[512,384]{1,0:T(8,128)(2,1)S(1)} fusion(bf16[512,2048]{1,0:T(8,128)(2,1)} %all-gather.2.cloned.1.call-done, bf16[2048,384]{1,0:T(8,128)(2,1)} %param.8), kind=kOutput, calls=%fused_computation.29 | convolution fusion | flops 805502976 | bytes 4063232 | tf_op jit(solution)/shard_map/dot_general | solution.py:63
  41.7 0.2 copy.39
  41.9 1.3 %gather_fusion = bf16[16,32,384]{2,1,0:T(8,128)(2,1)} fusion(bf16[16,32,384]{2,1,0:T(8,128)(2,1)S(1)} %bitcast.62, s32[1024]{0:T(1024)S(1)} %pad_clamp_fusion), kind=kCustom, calls=%fused_computation | custom fusion | bytes 786496 | tf_op jit(solution)/shard_map/gather | solution.py:91
  43.3 5.5 %all-to-all-start.1 = ((bf16[16,32,384]{2,1,0:T(8,128)(2,1)}), bf16[16,32,384]{2,1,0:T(8,128)(2,1)S(1)}, u32[]{:S(2)}, u32[]{:S(2)}) async-start(bf16[16,32,384]{2,1,0:T(8,128)(2,1)} %gather_fusion), calls=%async_computation.1 | async-start | bytes 786432 | tf_op jit(solution)/shard_map/all_to_all | solution.py:94
  48.8 1.4 %gather_fusion.1 = bf16[16,32,384]{2,1,0:T(8,128)(2,1)} fusion(bf16[16,32,384]{2,1,0:T(8,128)(2,1)S(1)} %bitcast.61, s32[1024]{0:T(1024)S(1)} %pad_clamp_fusion), kind=kCustom, calls=%fused_computation.1 | custom fusion | bytes 786496 | tf_op jit(solution)/shard_map/gather | solution.py:92
  50.2 3.1 %convolution_convert_fusion.3 = bf16[512,384]{0,1:T(8,128)(2,1)S(1)} fusion(bf16[512,2048]{1,0:T(8,128)(2,1)} %all-gather.2.cloned.1.call-done, bf16[2048,384]{1,0:T(8,128)(2,1)} %param.7), kind=kOutput, calls=%fused_computation.30 | convolution fusion | flops 805502976 | bytes 4063232 | tf_op jit(solution)/shard_map/dot_general | solution.py:63
  53.2 0.0 copy-start.4
  53.2 0.8 fusion
  54.0 0.0 copy-start.1
  54.1 1.7 %copy-done.1 = f32[3,512,512]{1,2,0:T(8,128)} copy-done((f32[3,512,512]{1,2,0:T(8,128)}, f32[3,512,512]{1,2,0:T(8,128)S(1)}, u32[]{:S(2)}) %copy-start.1) | copy-done | bytes 3145752
  55.7 0.8 fusion.2
  56.5 4.3 %all-to-all-done.1 = bf16[16,32,384]{2,1,0:T(8,128)(2,1)S(1)} async-done(((bf16[16,32,384]{2,1,0:T(8,128)(2,1)}), bf16[16,32,384]{2,1,0:T(8,128)(2,1)S(1)}, u32[]{:S(2)}, u32[]{:S(2)}) %all-to-all-start.1) | async-done | bytes 393248 | tf_op jit(solution)/shard_map/all_to_all | solution.py:94
  60.9 3.6 %all-to-all-start.2 = ((bf16[16,32,384]{2,1,0:T(8,128)(2,1)}), bf16[16,32,384]{2,1,0:T(8,128)(2,1)S(1)}, u32[]{:S(2)}, u32[]{:S(2)}) async-start(bf16[16,32,384]{2,1,0:T(8,128)(2,1)} %gather_fusion.1), calls=%async_computation.2 | async-start | bytes 786432 | tf_op jit(solution)/shard_map/all_to_all | solution.py:95
  64.5 0.0 copy-done.4
  64.5 0.2 reduce-scatter.2.cloned.1.call-start
  64.7 0.1 reshape_reshape.6
  64.8 0.0 copy-start.2
  64.9 0.0 copy-start.5
  64.9 1.9 %fusion.1 = (f32[3,512]{1,0:T(4,128)S(1)}, f32[3,512,512]{1,2,0:T(8,128)S(1)}) fusion(pred[512,512]{0,1:T(8,128)(4,1)S(1)} %get-tuple-element.12, bf16[512,3,128]{0,2,1:T(8,128)(2,1)} %bitcast.64, bf16[512,3,128]{2,1,0:T(4,128)(2,1)S(1)} %reshape_reshape.6), kind=kOutput, calls=%fused_computation.8 | convolution fusion | flops 203684352 | bytes 4200448 | tf_op jit(solution)/shard_map/qhd,khd->hqk/dot_general | solution.py:34
  66.8 0.0 copy-start.3
  66.8 1.7 %copy-done.3 = f32[3,512,512]{1,2,0:T(8,128)} copy-done((f32[3,512,512]{1,2,0:T(8,128)}, f32[3,512,512]{1,2,0:T(8,128)S(1)}, u32[]{:S(2)}) %copy-start.3) | copy-done | bytes 3145752
  68.5 0.8 fusion.4
  69.3 0.0 copy-done.2
  69.3 0.0 copy-done.5
  69.3 1.9 %fusion.18 = f32[512,3,128]{0,2,1:T(8,128)} fusion(bf16[512,3,128]{0,2,1:T(8,128)(2,1)S(1)} %bitcast.65, f32[3,512,512]{1,2,0:T(8,128)S(1)} %copy-done.2, f32[3,512]{1,0:T(4,128)S(1)} %get-tuple-element.16, pred[512,512]{0,1:T(8,128)(4,1)S(1)} %get-tuple-element.13, f32[512,3]{0,1:T(4,128)S(1)} %get-tuple-element.9), kind=kOutput, calls=%fused_computation.25 | convolution fusion | flops 204668928 | bytes 4599808 | tf_op jit(solution)/shard_map/hqk,khd->hqd/dot_general | solution.py:41
  71.2 5.2 %all-to-all-done.2 = bf16[16,32,384]{2,1,0:T(8,128)(2,1)S(1)} async-done(((bf16[16,32,384]{2,1,0:T(8,128)(2,1)}), bf16[16,32,384]{2,1,0:T(8,128)(2,1)S(1)}, u32[]{:S(2)}, u32[]{:S(2)}) %all-to-all-start.2) | async-done | bytes 393248 | tf_op jit(solution)/shard_map/all_to_all | solution.py:95
  76.4 0.1 reshape_reshape.7
  76.5 3.1 %fusion.22 = bf16[512,3,128]{0,2,1:T(8,128)(2,1)S(1)} fusion(f32[512,3,128]{0,2,1:T(8,128)} %fusion.18, f32[3,512,512]{1,2,0:T(8,128)} %copy-done.3, f32[3,512]{1,0:T(4,128)S(1)} %get-tuple-element.18, pred[512,512]{0,1:T(8,128)(4,1)S(1)} %get-tuple-element.12, bf16[512,3,128]{2,1,0:T(4,128)(2,1)S(1)} %reshape_reshape.7, ...), kind=kOutput, calls=%fused_computation.34 | convolution fusion | flops 205258752 | bytes 4999168 | tf_op jit(solution)/shard_map/hqk,khd->hqd/dot_general | solution.py:41
  79.6 0.0 copy-done
  79.6 2.7 %convolution_convert_fusion = bf16[512,2048]{1,0:T(8,128)(2,1)} fusion(bf16[512,384]{0,1:T(8,128)(2,1)S(1)} %bitcast.66, bf16[384,2048]{1,0:T(8,128)(2,1)S(1)} %copy-done), kind=kOutput, calls=%fused_computation.6 | convolution fusion | flops 806354944 | bytes 4063232 | tf_op jit(solution)/shard_map/dot_general | solution.py:111
  82.2 0.0 reduce-scatter.2.cloned.1.call-update
  82.3 29.4 %reduce-scatter.2.cloned.1.call-done = bf16[128,2048]{1,0:T(8,128)(2,1)} async-done(((bf16[512,2048]{1,0:T(8,128)(2,1)}), bf16[128,2048]{1,0:T(8,128)(2,1)}) %reduce-scatter.2.cloned.1.call-update) | async-done | bytes 524304 | tf_op jit(solution)/shard_map/reduce_scatter | solution.py:110
  (14 shorter events, 0.1 us)
Async XLA Ops:
  6.5 73.0 %copy-start = (bf16[384,2048]{1,0:T(8,128)(2,1)S(1)}, bf16[384,2048]{1,0:T(8,128)(2,1)}, u32[]{:S(2)}) copy-start(bf16[384,2048]{1,0:T(8,128)(2,1)} %param.10) | copy-start | bytes 4718596
  6.5 27.7 %all-gather.2.cloned.1.call-start = ((), (), s32[]{:S(2)}) async-start(), calls=%async_computation.4 | async-start | bytes 2621440 | tf_op jit(solution)/shard_map/all_gather | solution.py:59
  9.4 14.8 %all-to-all-start = ((s32[8,1,2]{2,1,0:T(1,128)}), s32[8,1,2]{2,1,0:T(1,128)S(1)}, u32[]{:S(2)}, u32[]{:S(2)}) async-start(s32[8,1,2]{2,1,0:T(1,128)} %copy.46), calls=%async_computation | async-start | bytes 8192 | tf_op jit(solution)/shard_map/all_to_all | solution.py:89
  43.3 17.6 %all-to-all-start.1 = ((bf16[16,32,384]{2,1,0:T(8,128)(2,1)}), bf16[16,32,384]{2,1,0:T(8,128)(2,1)S(1)}, u32[]{:S(2)}, u32[]{:S(2)}) async-start(bf16[16,32,384]{2,1,0:T(8,128)(2,1)} %gather_fusion), calls=%async_computation.1 | async-start | bytes 786432 | tf_op jit(solution)/shard_map/all_to_all | solution.py:94
  53.2 11.3 %copy-start.4 = (bf16[512,384]{0,1:T(8,128)(2,1)}, bf16[512,384]{0,1:T(8,128)(2,1)S(1)}, u32[]{:S(2)}) copy-start(bf16[512,384]{0,1:T(8,128)(2,1)S(1)} %convolution_convert_fusion.3) | copy-start | bytes 1179652
  54.0 1.7 %copy-start.1 = (f32[3,512,512]{1,2,0:T(8,128)}, f32[3,512,512]{1,2,0:T(8,128)S(1)}, u32[]{:S(2)}) copy-start(f32[3,512,512]{1,2,0:T(8,128)S(1)} %get-tuple-element.17) | copy-start | bytes 9437188
  60.9 15.5 %all-to-all-start.2 = ((bf16[16,32,384]{2,1,0:T(8,128)(2,1)}), bf16[16,32,384]{2,1,0:T(8,128)(2,1)S(1)}, u32[]{:S(2)}, u32[]{:S(2)}) async-start(bf16[16,32,384]{2,1,0:T(8,128)(2,1)} %gather_fusion.1), calls=%async_computation.2 | async-start | bytes 786432 | tf_op jit(solution)/shard_map/all_to_all | solution.py:95
  64.5 47.2 %reduce-scatter.2.cloned.1.call-start = ((), (), s32[]{:S(2)}) async-start(), calls=%async_computation.5 | async-start | bytes 2621440 | tf_op jit(solution)/shard_map/reduce_scatter | solution.py:110
  64.8 4.5 %copy-start.2 = (f32[3,512,512]{1,2,0:T(8,128)S(1)}, f32[3,512,512]{1,2,0:T(8,128)}, u32[]{:S(2)}) copy-start(f32[3,512,512]{1,2,0:T(8,128)} %copy-done.1) | copy-start | bytes 9437188
  64.9 4.5 %copy-start.5 = (bf16[512,384]{0,1:T(8,128)(2,1)S(1)}, bf16[512,384]{0,1:T(8,128)(2,1)}, u32[]{:S(2)}) copy-start(bf16[512,384]{0,1:T(8,128)(2,1)} %copy.42) | copy-start | bytes 1179652
  66.8 1.7 %copy-start.3 = (f32[3,512,512]{1,2,0:T(8,128)}, f32[3,512,512]{1,2,0:T(8,128)S(1)}, u32[]{:S(2)}) copy-start(f32[3,512,512]{1,2,0:T(8,128)S(1)} %get-tuple-element.19) | copy-start | bytes 9437188
Sparse Core Ops, SparseCore 0:
  8.9 25.2 all-gather.1
  82.4 29.2 reduce-scatter.1
where the time goes:
time: 119 us
  waiting for transfers between devices  49.5 us (42%)
  matrix products  19.9 us (17%)
  starting transfers between devices  16.7 us (14%)
  local copies, waits for them, and re-layouts  13.7 us (12%)
  between operations  13.6 us (11%)
  other arithmetic  5.12 us (4%)
    reduce_scatter x1, waiting for transfers between devices, local(): lax.psum_scatter(jnp.dot(rows, w_out, preferred_element_type=jnp.float32)...  29.4 us
    all_gather x1, waiting for transfers between devices, local(): piece = lax.all_gather(tokens, 'tp', axis=1, tiled=True)  9.83 us
    dot_general x3, matrix products, local(): outputs.append(jnp.dot(piece, rows, preferred_element_type=jnp.float32))  9.62 us
    all_to_all x1, starting transfers between devices, local(): lax.all_to_all(request, 'kv', split_axis=0, concat_axis=0, tiled=True)  7.31 us
    all_to_all x1, starting transfers between devices, local(): lax.all_to_all(send_keys, 'kv', split_axis=0, concat_axis=0, tiled=True)  5.51 us
    all_to_all x1, waiting for transfers between devices, local(): lax.all_to_all(send_values, 'kv', split_axis=0, concat_axis=0, tiled=True)  5.16 us
    dot_general x2, matrix products, attend(): jnp.einsum('hqk,khd->hqd', weights, value_heads.astype(jnp.float32))  4.96 us
    all_to_all x1, waiting for transfers between devices, local(): lax.all_to_all(send_keys, 'kv', split_axis=0, concat_axis=0, tiled=True)  4.32 us
  transfers between devices with their start and end apart: 5, of which 4 were waited for; matrix products, arithmetic and copies ran while one was open for 17% of the time, Pallas kernels for 0%

commit v1 on v0

v1 whole, which is shorter than its diff:
```python
import functools

import jax
import jax.numpy as jnp
from jax import lax
from jax.experimental import pallas as pl
from jax.experimental.pallas import tpu as pltpu
from jax.sharding import PartitionSpec as P

HD = 128
BLK = 32
MOST = 2
NEG = -1e30
BF = jnp.bfloat16
F32 = jnp.float32
MESH = pl.DeviceIdType.MESH
OWN_CHUNKS = 4
OUT_CHUNKS = 4


def dot(a, b):
    return jnp.dot(a, b, preferred_element_type=F32)


def dot_nt(a, b):
    return lax.dot_general(a, b, (((1,), (1,)), ((), ())), preferred_element_type=F32)


def iota(shape, dim):
    return lax.broadcasted_iota(jnp.int32, shape, dim)


def kernel(
    n, tok, wq, wk, wv, wo, chosen, out,
    wbuf, wobuf, gat, far, pick, ask, asked, acc, accf, qb, kb, vb, kf, vf,
    bias, biasf, top, tot, summed, att, hold, psend, precv, xsend, xrecv, mine,
    wsem, ox_s, ox_r, oc_s, oc_r, of_s, of_r, rq_s, rq_r, fk_s, fk_r,
    fx_s, fx_r, fc_s, fc_r, ff_s, ff_r, pd_s, pd_r, px_s, px_r,
):
    rows, feat = tok.shape
    width = wq.shape[1]
    heads = width // HD
    per = rows // BLK
    blocks = n * per
    slot = MOST * BLK
    cols = wo.shape[1]
    quarter = rows // 4
    me = lax.axis_index("kv")
    t = lax.axis_index("tp")
    mate = t + 1 - 2 * lax.rem(t, 2)
    across = lax.rem(t + 2, 4)
    diag = lax.rem(mate + 2, 4)
    order = (t, mate, across, diag)

    loads = []
    for d in range(4):
        for j, w in enumerate((wq, wk, wv)):
            src = pl.ds(pl.multiple_of(order[d] * feat, feat), feat)
            c = pltpu.make_async_copy(w.at[src, :], wbuf.at[j, d], wsem.at[d * 3 + j])
            c.start()
            loads.append(c)
    wo_load = pltpu.make_async_copy(wo, wobuf, wsem.at[12])
    wo_load.start()

    barrier = pltpu.get_barrier_semaphore()
    for d in range(1, 4):
        pl.semaphore_signal(barrier, inc=1, device_id=(me, order[d]), device_id_type=MESH)
    for k in range(1, n):
        pl.semaphore_signal(
            barrier, inc=1, device_id=(lax.rem(me + k, n), t), device_id_type=MESH
        )
    pl.semaphore_wait(barrier, n + 2)

    def remote(src, dst, s, r, who):
        c = pltpu.make_async_remote_copy(
            src_ref=src, dst_ref=dst, send_sem=s, recv_sem=r, device_id=who, device_id_type=MESH
        )
        return c

    piece = rows // OWN_CHUNKS
    own_x = []
    for c in range(OWN_CHUNKS):
        part = pl.ds(c * piece, piece)
        own_x.append(
            remote(tok.at[part], gat.at[1, part], ox_s.at[c], ox_r.at[c], (me, across))
        )
        own_x[-1].start()
    own_c = remote(tok, gat.at[0], oc_s, oc_r, (me, mate))
    own_c.start()

    lane = iota((per, blocks), 1)
    seen = jnp.zeros((per, blocks), jnp.int32)
    picks = chosen[...]
    for j in range(picks.shape[1]):
        seen = jnp.maximum(seen, (picks[:, j : j + 1] == lane).astype(jnp.int32))
    wanted = jnp.max(seen, axis=0, keepdims=True)
    lane1 = iota((1, blocks), 1)
    inside = (lane1 >= me * per) & (lane1 < me * per + per)
    wanted = jnp.where(inside, 0, wanted)
    ask[...] = jnp.broadcast_to(wanted, (8, blocks))
    asks = []
    for k in range(1, n):
        c = remote(
            ask, asked.at[k - 1], rq_s.at[k - 1], rq_r.at[k - 1], (lax.rem(me + n - k, n), t)
        )
        c.start()
        asks.append(c)

    ia, ib = iota((blocks, blocks), 0), iota((blocks, blocks), 1)
    tri = ((lax.div(ia, per) == lax.div(ib, per)) & (ia <= ib)).astype(BF)
    seen_b = seen.astype(F32).astype(BF)
    want8 = jnp.broadcast_to(wanted, (8, blocks)).astype(F32)
    rank8 = dot(want8.astype(BF), tri) * want8
    rank = rank8[0:1, :]
    spots = n * slot
    col = iota((spots, blocks), 0)
    blk = iota((spots, blocks), 1)
    away = me - lax.div(blk, per)
    away = jnp.where(away < 0, away + n, away)
    hit = (lax.div(col, slot) == away - 1) & (
        jnp.broadcast_to(rank, (spots, blocks))
        == (lax.div(lax.rem(col, slot), BLK) + 1).astype(F32)
    )
    hit = hit.astype(F32).astype(BF)
    far_seen = dot_nt(seen_b, hit)
    grow = (lax.div(iota((rows, per), 0), BLK) == iota((rows, per), 1)).astype(F32).astype(BF)
    biasf[...] = jnp.where(dot(grow, far_seen.astype(BF)) > 0.5, 0.0, NEG)
    spread = (
        (iota((blocks, rows), 0) == me * per + lax.div(iota((blocks, rows), 1), BLK))
        .astype(F32)
        .astype(BF)
    )
    own_seen = dot(grow, dot(seen_b, spread).astype(BF))
    causal = iota((rows, rows), 1) <= iota((rows, rows), 0)
    bias[...] = jnp.where((own_seen > 0.5) & causal, 0.0, NEG)

    for c in asks:
        c.wait_recv()
    others = asked[:, 0, :].astype(F32)
    ranks = dot(others.astype(BF), tri) * others
    places = dot(ranks.astype(BF), spread)
    srow, scol = iota((slot, rows), 0), iota((slot, rows), 1)
    same = lax.rem(srow, BLK) == lax.rem(scol, BLK)
    want_rank = (lax.div(srow, BLK) + 1).astype(F32)
    sends = []
    for k in range(1, n):
        sel = same & (jnp.broadcast_to(places[k - 1 : k, :], (slot, rows)) == want_rank)
        pick[k - 1] = dot(sel.astype(F32).astype(BF), tok[...]).astype(BF)
        c = remote(
            pick.at[k - 1],
            far.at[0, pl.ds((k - 1) * slot, slot)],
            fk_s.at[k - 1],
            fk_r.at[k - 1],
            (lax.rem(me + k, n), t),
        )
        c.start()
        sends.append(c)

    half = rows // 2

    def project(d, src, first):
        for c in loads[3 * d : 3 * d + 3]:
            c.wait()
        for j in range(3):
            for r in range(2):
                part = pl.ds(r * half, half)
                val = dot(src[part, :], wbuf[j, d])
                if first:
                    acc[j, part, :] = val
                else:
                    acc[j, part, :] += val

    project(0, tok, True)
    own_c.wait_recv()
    project(1, gat.at[0], False)

    fwd = []
    for c in range(OWN_CHUNKS):
        own_x[c].wait_recv()
        part = pl.ds(c * piece, piece)
        f = remote(gat.at[1, part], gat.at[2, part], of_s.at[c], of_r.at[c], (me, mate))
        f.start()
        fwd.append(f)

    far_x, far_c = [], []
    for k in range(1, n):
        part = pl.ds((k - 1) * slot, slot)
        sends[k - 1].wait_recv()
        c = remote(far.at[0, part], far.at[2, part], fx_s.at[k - 1], fx_r.at[k - 1], (me, across))
        c.start()
        far_x.append(c)
        c = remote(far.at[0, part], far.at[1, part], fc_s.at[k - 1], fc_r.at[k - 1], (me, mate))
        c.start()
        far_c.append(c)

    project(2, gat.at[1], False)
    for f in fwd:
        f.wait_recv()
    project(3, gat.at[2], False)
    qb[...] = acc[0].astype(BF)
    kb[...] = acc[1].astype(BF)
    vb[...] = acc[2].astype(BF)

    scale = HD ** (-0.5)
    step = rows // 4
    for h in range(heads):
        hc = slice(h * HD, (h + 1) * HD)
        for r in range(4):
            rr = slice(r * step, (r + 1) * step)
            upto = (r + 1) * step
            s = dot_nt(qb[rr, hc], kb[:upto, hc]) * scale + bias[rr, :upto]
            m = jnp.max(s, axis=1, keepdims=True)
            p = jnp.exp(s - m)
            top[h, rr, :] = m
            tot[h, rr, :] = jnp.sum(p, axis=1, keepdims=True)
            summed[h, rr, :] = dot(p.astype(BF), vb[:upto, hc])

    far_f = []
    for k in range(1, n):
        part = pl.ds((k - 1) * slot, slot)
        far_x[k - 1].wait_recv()
        f = remote(far.at[2, part], far.at[3, part], ff_s.at[k - 1], ff_r.at[k - 1], (me, mate))
        f.start()
        far_f.append(f)
    used = (n - 1) * slot
    for c in far_c:
        c.wait_recv()
    for d in range(3):
        for j in range(2):
            val = dot(far[d], wbuf[1 + j, d])
            if d == 0:
                accf[j] = val
            else:
                accf[j] += val
    for c in far_f:
        c.wait_recv()
    for j, dst in enumerate((kf, vf)):
        dst[pl.ds(0, used), :] = (accf[j] + dot(far[3], wbuf[1 + j, 3])).astype(BF)
        dst[pl.ds(used, spots - used), :] = jnp.zeros((spots - used, width), BF)

    def finish(who):
        part = pl.ds(pl.multiple_of(who * quarter, quarter), quarter)
        for h in range(heads):
            hc = slice(h * HD, (h + 1) * HD)
            s = dot_nt(qb[part, hc], kf[:, hc]) * scale + biasf[part, :]
            m0 = top[h, part, :]
            m = jnp.maximum(m0, jnp.max(s, axis=1, keepdims=True))
            p = jnp.exp(s - m)
            keep = jnp.exp(m0 - m)
            total = tot[h, part, :] * keep + jnp.sum(p, axis=1, keepdims=True)
            val = summed[h, part, :] * keep + dot(p.astype(BF), vf[:, hc])
            att[part, hc] = (val / total).astype(BF)
        return part

    wo_load.wait()
    wide = cols // OUT_CHUNKS
    to_mate, to_across = [], []

    def share(which, who):
        part = finish(who)
        for c in range(OUT_CHUNKS):
            psend[which, c] = dot(att[part, :], wobuf[:, c * wide : (c + 1) * wide]).astype(BF)
            i = which * OUT_CHUNKS + c
            x = remote(
                psend.at[which, c], precv.at[which, c], pd_s.at[i], pd_r.at[i], (me, mate)
            )
            x.start()
            to_mate.append(x)

    share(0, diag)
    part = finish(across)
    for c in range(OUT_CHUNKS):
        val = dot(att[part, :], wobuf[:, c * wide : (c + 1) * wide])
        to_mate[c].wait_recv()
        xsend[c] = (val + precv[0, c].astype(F32)).astype(BF)
        x = remote(xsend.at[c], xrecv.at[c], px_s.at[c], px_r.at[c], (me, across))
        x.start()
        to_across.append(x)
    share(1, mate)
    part = finish(t)
    for c in range(OUT_CHUNKS):
        val = dot(att[part, :], wobuf[:, c * wide : (c + 1) * wide])
        to_mate[OUT_CHUNKS + c].wait_recv()
        mine[c] = val + precv[1, c].astype(F32)
    for c in range(OUT_CHUNKS):
        to_across[c].wait_recv()
        out[:, c * wide : (c + 1) * wide] = (mine[c] + xrecv[c].astype(F32)).astype(BF)

    for c in own_x + [own_c] + asks + sends + fwd + far_x + far_c + far_f + to_mate + to_across:
        c.wait_send()


def local(n, tokens, w_query, w_key, w_value, w_out, chosen):
    rows, feat = tokens.shape
    width = w_query.shape[1]
    heads = width // HD
    cols = w_out.shape[1]
    blocks = n * (rows // BLK)
    slot = MOST * BLK
    used, spots = (n - 1) * slot, n * slot
    quarter = rows // 4
    wide = cols // OUT_CHUNKS
    vmem = pl.BlockSpec(memory_space=pltpu.VMEM)
    hbm = pl.BlockSpec(memory_space=pl.ANY)
    dma = pltpu.SemaphoreType.DMA
    V = pltpu.VMEM
    return pl.pallas_call(
        functools.partial(kernel, n),
        out_shape=jax.ShapeDtypeStruct((quarter, cols), BF),
        in_specs=[vmem, hbm, hbm, hbm, hbm, vmem],
        out_specs=vmem,
        scratch_shapes=[
            V((3, 4, feat, width), BF),
            V((width, cols), BF),
            V((3, rows, feat), BF),
            V((4, used, feat), BF),
            V((n - 1, slot, feat), BF),
            V((8, blocks), jnp.int32),
            V((n - 1, 8, blocks), jnp.int32),
            V((3, rows, width), F32),
            V((2, used, width), F32),
            V((rows, width), BF),
            V((rows, width), BF),
            V((rows, width), BF),
            V((spots, width), BF),
            V((spots, width), BF),
            V((rows, rows), F32),
            V((rows, spots), F32),
            V((heads, rows, 1), F32),
            V((heads, rows, 1), F32),
            V((heads, rows, HD), F32),
            V((rows, width), BF),
            V((8, 128), F32),
            V((2, OUT_CHUNKS, quarter, wide), BF),
            V((2, OUT_CHUNKS, quarter, wide), BF),
            V((OUT_CHUNKS, quarter, wide), BF),
            V((OUT_CHUNKS, quarter, wide), BF),
            V((OUT_CHUNKS, quarter, wide), F32),
            dma((13,)),
            dma((OWN_CHUNKS,)), dma((OWN_CHUNKS,)),
            dma, dma,
            dma((OWN_CHUNKS,)), dma((OWN_CHUNKS,)),
            dma((n - 1,)), dma((n - 1,)),
            dma((n - 1,)), dma((n - 1,)),
            dma((n - 1,)), dma((n - 1,)),
            dma((n - 1,)), dma((n - 1,)),
            dma((n - 1,)), dma((n - 1,)),
            dma((2 * OUT_CHUNKS,)), dma((2 * OUT_CHUNKS,)),
            dma((OUT_CHUNKS,)), dma((OUT_CHUNKS,)),
        ],
        compiler_params=pltpu.CompilerParams(
            collective_id=0, has_side_effects=True, vmem_limit_bytes=60 * 1024 * 1024
        ),
    )(tokens, w_query, w_key, w_value, w_out, chosen)


def solution(mesh):
    return jax.shard_map(
        functools.partial(local, mesh.shape["kv"]),
        mesh=mesh,
        in_specs=(
            P("kv", "tp"),
            P(None, "tp"),
            P(None, "tp"),
            P(None, "tp"),
            P("tp", None),
            P("kv", None),
        ),
        out_specs=P(("kv", "tp"), None),
        check_vma=False,
    )
```

time: 119 us -> 53.6 us (0.45)
  Pallas kernels: 0 us -> 51.6 us
  waiting for transfers between devices: 49.5 us -> 0 us
  matrix products: 19.9 us -> 0 us
  starting transfers between devices: 16.7 us -> 0 us
  between operations: 13.6 us -> 0.01 us
  local copies, waits for them, and re-layouts: 13.7 us -> 1.88 us
  other arithmetic: 5.12 us -> 0 us
    pallas_call x0 -> x1, Pallas kernels: none -> 51.6 us  [local(): pl.pallas_call(functools.partial(kernel, n), out_shape=jax.ShapeDtypeStru...]
    reduce_scatter x1 -> x0, waiting for transfers between devices: 29.4 us -> none  [local(): lax.psum_scatter(jnp.dot(rows, w_out, preferred_element_type=jnp.float32)...]
    dot_general x8 -> x0, matrix products: 19.9 us -> none  [the longest x3 9.62 us: local(): outputs.append(jnp.dot(piece, rows, preferred_element_type=jnp.float32))]
    all_to_all x3 -> x0, starting transfers between devices: 16.5 us -> none  [the longest x1 7.31 us: local(): lax.all_to_all(request, 'kv', split_axis=0, concat_axis=0, tiled=True)]
    all_gather x1 -> x0, waiting for transfers between devices: 9.83 us -> none  [local(): piece = lax.all_gather(tokens, 'tp', axis=1, tiled=True)]
    all_to_all x3 -> x0, waiting for transfers between devices: 9.48 us -> none  [the longest x1 5.16 us: local(): lax.all_to_all(send_values, 'kv', split_axis=0, concat_axis=0, tiled=True)]
    reshape x3 -> x0, local copies, waits for them, and re-layouts: 4.3 us -> none  [the longest x2 4.21 us: attend(): jnp.broadcast_to(seen[:, None, :, None], (query_blocks, BLK, slot_count,...]
    gather x2 -> x0, local copies, waits for them, and re-layouts: 2.71 us -> none  [the longest x1 1.37 us: local(): send_values = value_rows.reshape(per_dev, BLK, width)[picked]]
  transfers between devices with their start and end apart: 5 -> 0, of which waited for: 4 -> 0; matrix products, arithmetic and copies ran while one was open for 17% -> 0% of each run, Pallas kernels for 0% -> 0%
where the time goes in v1:
time: 53.6 us; the launch traced here: 53.4 us
  Pallas kernels  51.6 us (96%)
  local copies, waits for them, and re-layouts  1.88 us (4%)
    pallas_call x1, Pallas kernels, local(): pl.pallas_call(functools.partial(kernel, n), out_shape=jax.ShapeDtypeStru...  51.6 us
    unnamed x1, local copies, waits for them, and re-layouts  1.88 us

profile of v1, /device:TPU:0, one launch (start us, length us, event | category | flops | bytes accessed | tf_op | source)
XLA Modules:
  0.0 53.4 jit_solution(16611471896592207186)
XLA Ops:
  0.0 51.6 %shard_map.64 = bf16[128,2048]{1,0:T(8,128)(2,1)} custom-call(bf16[512,512]{1,0:T(8,128)(2,1)} %tok.1, bf16[2048,384]{1,0:T(8,128)(2,1)} %wq.1, bf16[2048,384]{1,0:T(8,128)(2,1)} %wk.1, bf16[2048,384]{1,0:T(8,128)(2,1)} %wv.1, bf16[384,2048]{1,0:T(8,128)(2,1)} %wo.1, s32[16,24]{1,0:T(8,128)} %chosen.1), custom_call_target="tpu_custom_call" | custom-call | tf_op jit(solution)/shard_map/pallas_call | solution.py:307
  51.6 1.9 %copy.8 = bf16[128,2048]{1,0:T(8,128)(2,1)} copy(bf16[128,2048]{1,0:T(8,128)(2,1)} %shard_map.64) | data formatting | bytes 1048576

commit v2 on v1

--- a/solution.py
+++ b/solution.py
@@ -11,6 +11,7 @@
 BLK = 32
 MOST = 2
 NEG = -1e30
+LOG2E = 1.4426950408889634
 BF = jnp.bfloat16
 F32 = jnp.float32
 MESH = pl.DeviceIdType.MESH
@@ -26,6 +27,18 @@
     return lax.dot_general(a, b, (((1,), (1,)), ((), ())), preferred_element_type=F32)
 
 
+def quot(x, size):
+    if size & (size - 1) == 0:
+        return lax.shift_right_logical(x, jnp.full(x.shape, size.bit_length() - 1, x.dtype))
+    return lax.div(x, size)
+
+
+def rest(x, size):
+    if size & (size - 1) == 0:
+        return x & (size - 1)
+    return lax.rem(x, size)
+
+
 def iota(shape, dim):
     return lax.broadcasted_iota(jnp.int32, shape, dim)
 
@@ -33,7 +46,7 @@
 def kernel(
     n, tok, wq, wk, wv, wo, chosen, out,
     wbuf, wobuf, gat, far, pick, ask, asked, acc, accf, qb, kb, vb, kf, vf,
-    bias, biasf, top, tot, summed, att, hold, psend, precv, xsend, xrecv, mine,
+    bias, biasf, top, tot, summed, att, psend, precv, xsend, xrecv, mine,
     wsem, ox_s, ox_r, oc_s, oc_r, of_s, of_r, rq_s, rq_r, fk_s, fk_r,
     fx_s, fx_r, fc_s, fc_r, ff_s, ff_r, pd_s, pd_r, px_s, px_r,
 ):
@@ -107,41 +120,24 @@
         asks.append(c)
 
     ia, ib = iota((blocks, blocks), 0), iota((blocks, blocks), 1)
-    tri = ((lax.div(ia, per) == lax.div(ib, per)) & (ia <= ib)).astype(BF)
+    tri = ((quot(ia, per) == quot(ib, per)) & (ia <= ib)).astype(BF)
     seen_b = seen.astype(F32).astype(BF)
     want8 = jnp.broadcast_to(wanted, (8, blocks)).astype(F32)
     rank8 = dot(want8.astype(BF), tri) * want8
     rank = rank8[0:1, :]
-    spots = n * slot
-    col = iota((spots, blocks), 0)
-    blk = iota((spots, blocks), 1)
-    away = me - lax.div(blk, per)
-    away = jnp.where(away < 0, away + n, away)
-    hit = (lax.div(col, slot) == away - 1) & (
-        jnp.broadcast_to(rank, (spots, blocks))
-        == (lax.div(lax.rem(col, slot), BLK) + 1).astype(F32)
-    )
-    hit = hit.astype(F32).astype(BF)
-    far_seen = dot_nt(seen_b, hit)
-    grow = (lax.div(iota((rows, per), 0), BLK) == iota((rows, per), 1)).astype(F32).astype(BF)
-    biasf[...] = jnp.where(dot(grow, far_seen.astype(BF)) > 0.5, 0.0, NEG)
     spread = (
-        (iota((blocks, rows), 0) == me * per + lax.div(iota((blocks, rows), 1), BLK))
+        (iota((blocks, rows), 0) == me * per + quot(iota((blocks, rows), 1), BLK))
         .astype(F32)
         .astype(BF)
     )
-    own_seen = dot(grow, dot(seen_b, spread).astype(BF))
-    causal = iota((rows, rows), 1) <= iota((rows, rows), 0)
-    bias[...] = jnp.where((own_seen > 0.5) & causal, 0.0, NEG)
-
     for c in asks:
         c.wait_recv()
     others = asked[:, 0, :].astype(F32)
     ranks = dot(others.astype(BF), tri) * others
     places = dot(ranks.astype(BF), spread)
     srow, scol = iota((slot, rows), 0), iota((slot, rows), 1)
-    same = lax.rem(srow, BLK) == lax.rem(scol, BLK)
-    want_rank = (lax.div(srow, BLK) + 1).astype(F32)
+    same = rest(srow, BLK) == rest(scol, BLK)
+    want_rank = (quot(srow, BLK) + 1).astype(F32)
     sends = []
     for k in range(1, n):
         sel = same & (jnp.broadcast_to(places[k - 1 : k, :], (slot, rows)) == want_rank)
@@ -171,19 +167,37 @@
                     acc[j, part, :] += val
 
     project(0, tok, True)
+    spots = n * slot
+    col = iota((spots, blocks), 0)
+    blk = iota((spots, blocks), 1)
+    away = me - quot(blk, per)
+    away = jnp.where(away < 0, away + n, away)
+    hit = (quot(col, slot) == away - 1) & (
+        jnp.broadcast_to(rank, (spots, blocks))
+        == (quot(rest(col, slot), BLK) + 1).astype(F32)
+    )
+    hit = hit.astype(F32).astype(BF)
+    far_seen = dot_nt(seen_b, hit)
+    grow = (quot(iota((rows, per), 0), BLK) == iota((rows, per), 1)).astype(F32).astype(BF)
+    biasf[...] = jnp.where(dot(grow, far_seen.astype(BF)) > 0.5, 0.0, NEG)
+    own_seen = dot(grow, dot(seen_b, spread).astype(BF))
+    causal = iota((rows, rows), 1) <= iota((rows, rows), 0)
+    bias[...] = jnp.where((own_seen > 0.5) & causal, 0.0, NEG)
+
+
     own_c.wait_recv()
     project(1, gat.at[0], False)
 
-    fwd = []
-    for c in range(OWN_CHUNKS):
+    fwd, far_x, far_c = [], [], []
+
+    def hand_own(c):
         own_x[c].wait_recv()
         part = pl.ds(c * piece, piece)
         f = remote(gat.at[1, part], gat.at[2, part], of_s.at[c], of_r.at[c], (me, mate))
         f.start()
         fwd.append(f)
 
-    far_x, far_c = [], []
-    for k in range(1, n):
+    def hand_far(k):
         part = pl.ds((k - 1) * slot, slot)
         sends[k - 1].wait_recv()
         c = remote(far.at[0, part], far.at[2, part], fx_s.at[k - 1], fx_r.at[k - 1], (me, across))
@@ -193,6 +207,12 @@
         c.start()
         far_c.append(c)
 
+    for k in range(1, n):
+        hand_far(k)
+        at = k * OWN_CHUNKS // (n - 1)
+        for c in range((k - 1) * OWN_CHUNKS // (n - 1), at):
+            hand_own(c)
+
     project(2, gat.at[1], False)
     for f in fwd:
         f.wait_recv()
@@ -201,37 +221,43 @@
     kb[...] = acc[1].astype(BF)
     vb[...] = acc[2].astype(BF)
 
-    scale = HD ** (-0.5)
+    scale = HD ** (-0.5) * LOG2E
     step = rows // 4
-    for h in range(heads):
-        hc = slice(h * HD, (h + 1) * HD)
-        for r in range(4):
-            rr = slice(r * step, (r + 1) * step)
-            upto = (r + 1) * step
-            s = dot_nt(qb[rr, hc], kb[:upto, hc]) * scale + bias[rr, :upto]
-            m = jnp.max(s, axis=1, keepdims=True)
-            p = jnp.exp(s - m)
-            top[h, rr, :] = m
-            tot[h, rr, :] = jnp.sum(p, axis=1, keepdims=True)
-            summed[h, rr, :] = dot(p.astype(BF), vb[:upto, hc])
-
-    far_f = []
-    for k in range(1, n):
-        part = pl.ds((k - 1) * slot, slot)
-        far_x[k - 1].wait_recv()
-        f = remote(far.at[2, part], far.at[3, part], ff_s.at[k - 1], ff_r.at[k - 1], (me, mate))
-        f.start()
-        far_f.append(f)
-    used = (n - 1) * slot
-    for c in far_c:
-        c.wait_recv()
-    for d in range(3):
+    cut = [slice(h * HD, (h + 1) * HD) for h in range(heads)]
+    for r in range(4):
+        rr = slice(r * step, (r + 1) * step)
+        upto = (r + 1) * step
+        shade = bias[rr, :upto]
+        ss = [dot_nt(qb[rr, hc], kb[:upto, hc]) * scale + shade for hc in cut]
+        ms = [jnp.max(x, axis=1, keepdims=True) for x in ss]
+        ps = [jnp.exp2(x - m) for x, m in zip(ss, ms)]
+        vals = [dot(p.astype(BF), vb[:upto, hc]) for p, hc in zip(ps, cut)]
+        for h in range(heads):
+            top[h, rr, :] = ms[h]
+            tot[h, rr, :] = jnp.sum(ps[h], axis=1, keepdims=True)
+            summed[h, rr, :] = vals[h]
+
+    def project_far(d):
         for j in range(2):
             val = dot(far[d], wbuf[1 + j, d])
             if d == 0:
                 accf[j] = val
             else:
                 accf[j] += val
+
+    project_far(0)
+    for c in far_c:
+        c.wait_recv()
+    project_far(1)
+    far_f = []
+    used = (n - 1) * slot
+    for k in range(1, n):
+        part = pl.ds((k - 1) * slot, slot)
+        far_x[k - 1].wait_recv()
+        f = remote(far.at[2, part], far.at[3, part], ff_s.at[k - 1], ff_r.at[k - 1], (me, mate))
+        f.start()
+        far_f.append(f)
+    project_far(2)
     for c in far_f:
         c.wait_recv()
     for j, dst in enumerate((kf, vf)):
@@ -240,16 +266,17 @@
 
     def finish(who):
         part = pl.ds(pl.multiple_of(who * quarter, quarter), quarter)
+        shade = biasf[part, :]
+        ss = [dot_nt(qb[part, hc], kf[:, hc]) * scale + shade for hc in cut]
+        old = [top[h, part, :] for h in range(heads)]
+        ms = [jnp.maximum(m, jnp.max(x, axis=1, keepdims=True)) for m, x in zip(old, ss)]
+        ps = [jnp.exp2(x - m) for x, m in zip(ss, ms)]
+        keep = [jnp.exp2(m0 - m) for m0, m in zip(old, ms)]
+        vals = [dot(p.astype(BF), vf[:, hc]) for p, hc in zip(ps, cut)]
         for h in range(heads):
-            hc = slice(h * HD, (h + 1) * HD)
-            s = dot_nt(qb[part, hc], kf[:, hc]) * scale + biasf[part, :]
-            m0 = top[h, part, :]
-            m = jnp.maximum(m0, jnp.max(s, axis=1, keepdims=True))
-            p = jnp.exp(s - m)
-            keep = jnp.exp(m0 - m)
-            total = tot[h, part, :] * keep + jnp.sum(p, axis=1, keepdims=True)
-            val = summed[h, part, :] * keep + dot(p.astype(BF), vf[:, hc])
-            att[part, hc] = (val / total).astype(BF)
+            total = tot[h, part, :] * keep[h] + jnp.sum(ps[h], axis=1, keepdims=True)
+            val = summed[h, part, :] * keep[h] + vals[h]
+            att[part, cut[h]] = (val / total).astype(BF)
         return part
 
     wo_load.wait()
@@ -301,7 +328,7 @@
     quarter = rows // 4
     wide = cols // OUT_CHUNKS
     vmem = pl.BlockSpec(memory_space=pltpu.VMEM)
-    hbm = pl.BlockSpec(memory_space=pl.ANY)
+    hbm = pl.BlockSpec(memory_space=pltpu.HBM)
     dma = pltpu.SemaphoreType.DMA
     V = pltpu.VMEM
     return pl.pallas_call(
@@ -330,7 +357,6 @@
             V((heads, rows, 1), F32),
             V((heads, rows, HD), F32),
             V((rows, width), BF),
-            V((8, 128), F32),
             V((2, OUT_CHUNKS, quarter, wide), BF),
             V((2, OUT_CHUNKS, quarter, wide), BF),
             V((OUT_CHUNKS, quarter, wide), BF),

time: 53.6 us -> 51.6 us (0.963)
  Pallas kernels: 51.6 us -> 49.5 us
    pallas_call x1, Pallas kernels: 51.6 us -> 49.5 us  [local(): pl.pallas_call(functools.partial(kernel, n), out_shape=jax.ShapeDtypeStru...]
where the time goes in v2:
time: 51.6 us; the launch traced here: 51.4 us
  Pallas kernels  49.5 us (96%)
  local copies, waits for them, and re-layouts  1.88 us (4%)
    pallas_call x1, Pallas kernels, local(): pl.pallas_call(functools.partial(kernel, n), out_shape=jax.ShapeDtypeStru...  49.5 us
    unnamed x1, local copies, waits for them, and re-layouts  1.88 us

profile of v2, /device:TPU:0, one launch (start us, length us, event | category | flops | bytes accessed | tf_op | source)
XLA Modules:
  0.0 51.4 jit_solution(8429186671043239397)
XLA Ops:
  0.0 49.5 %shard_map.64 = bf16[128,2048]{1,0:T(8,128)(2,1)} custom-call(bf16[512,512]{1,0:T(8,128)(2,1)} %tok.1, bf16[2048,384]{1,0:T(8,128)(2,1)} %wq.1, bf16[2048,384]{1,0:T(8,128)(2,1)} %wk.1, bf16[2048,384]{1,0:T(8,128)(2,1)} %wv.1, bf16[384,2048]{1,0:T(8,128)(2,1)} %wo.1, s32[16,24]{1,0:T(8,128)} %chosen.1), custom_call_target="tpu_custom_call" | custom-call | tf_op jit(solution)/shard_map/pallas_call | solution.py:334
  49.5 1.9 %copy.8 = bf16[128,2048]{1,0:T(8,128)(2,1)} copy(bf16[128,2048]{1,0:T(8,128)(2,1)} %shard_map.64) | data formatting | bytes 1048576
